TPU v7x, 256 devices: a whole 4x4x8 slice. The times are simulated.
256 devices in a mesh: sp: 64 (over z, x, core), tp: 4 (over y).
Axes of the slice: x: 4, y: 4, z: 8, core: 2. Of those that a mesh axis runs over, the one named last changes fastest.
Arguments:
- x_in: bfloat16 [32768, 1024], P('sp', 'tp'), may hold values from -6 to 6
- gate_b: bfloat16 [32768, 1024], P('sp', 'tp'), may hold values from -6 to 6
- gate_c: bfloat16 [32768, 1024], P('sp', 'tp'), may hold values from -6 to 6
- conv_taps: bfloat16 [3, 1024], P(None, 'tp'), may hold values from -3.5 to 3.5
- out_proj: bfloat16 [1024, 2048], P('tp'), may hold values from -0.1875 to 0.1875
- mix_gain: bfloat16 [2048], replicated, may hold values from 0.099609375 to 1.8984375
- resid: bfloat16 [32768, 2048], P(('sp', 'tp')), may hold values from -6 to 6
- pre_gain: bfloat16 [2048], replicated, may hold values from 0.099609375 to 1.8984375
- expert_gate: bfloat16 [64, 2048, 512], P('sp'), may hold values from -0.125 to 0.125
- expert_up: bfloat16 [64, 2048, 512], P('sp'), may hold values from -0.125 to 0.125
- expert_down: bfloat16 [64, 512, 2048], P('sp'), may hold values from -7.1594562 to 7.1594562
- shared_gate: bfloat16 [2048, 256], replicated, may hold values from -0.125 to 0.125
- shared_up: bfloat16 [2048, 256], replicated, may hold values from -0.125 to 0.125
- shared_down: bfloat16 [256, 2048], replicated, may hold values from -10.125 to 10.125
- post_gain: bfloat16 [2048], replicated, may hold values from 0.099609375 to 1.8984375
- routes: int32 [32768, 4], P(('sp', 'tp')), may hold values from 0 to 63, all different within a row; in each aligned block of 128 rows (0 to 127, 128 to 255, ...) at most 12 rows name the same one
- route_weights: float32 [32768, 4], P(('sp', 'tp')), may hold values from 0.1 to 1
Outputs:
- layer_out: bfloat16 [32768, 2048], P(('sp', 'tp'))
Inputs may be any that keep to these rules, and one draw needn't show every extreme that they name: `routes`: each row names 4 different experts. Within the rows of one device (aligned blocks), no expert is named by more than 12 rows, and in some block one expert is named by exactly 12 rows.
All inputs are finite; a program needn't handle non-finite values.
Results may differ from a plain program's by a relative error of at most 0.007.
Values may be sent and summed in bfloat16 or wider, within the bound.
A program may use at most 128 MiB of HBM per device.

v0:
```python
import jax
import jax.numpy as jnp
from jax import lax
from jax.experimental import pallas as pl
from jax.experimental.pallas import tpu as pltpu
from jax.sharding import Mesh
from jax.sharding import PartitionSpec as P

SP = ("sp_0", "sp_1", "sp_2")
SP_TP = ("sp_0", "sp_1", "sp_2", "tp")
MESH = pl.DeviceIdType.MESH

epsilon = 1e-06

Z, X, C, Y = 8, 4, 2, 4
PLANE = X * C
CAP = 12
SIDE = 2
ROWS = SIDE * CAP
SLOTS = PLANE * ROWS
GROUPS = Z // 2
META = 256
TILE = 8
TILES = ROWS // TILE
STRIP = PLANE * TILE
LATE = 2
UNITS = 4


def row_of(ref):
    rows = ref[...].astype(jnp.float32)
    return jnp.concatenate([rows[i : i + 1] for i in range(rows.shape[0])], axis=1)


def fill_tables(meta, routes, route_weights):
    top, tokens = routes.shape
    f32, bf16 = jnp.float32, jnp.bfloat16
    experts = Z * PLANE
    expert = lax.broadcasted_iota(jnp.int32, (experts, tokens), 0)
    named = jnp.zeros((experts, tokens), f32)
    weight = jnp.zeros((experts, tokens), f32)
    for k in range(top):
        hot = expert == routes[k : k + 1]
        named = named + jnp.where(hot, 1.0, 0.0)
        weight = weight + jnp.where(hot, route_weights[k : k + 1], 0.0)
    named = named.T
    weight = weight.T
    row = lax.broadcasted_iota(jnp.int32, (tokens, tokens), 0)
    column = lax.broadcasted_iota(jnp.int32, (tokens, tokens), 1)
    below = jnp.where(row > column, 1.0, 0.0).astype(bf16)
    before = jnp.dot(below, named.astype(bf16), preferred_element_type=f32)
    place = jnp.where(named > 0.0, before, 100.0).astype(bf16)
    high = weight.astype(bf16)
    low = (weight - high.astype(f32)).astype(bf16)
    lane = lax.broadcasted_iota(jnp.int32, (experts, META), 1)
    expert = lax.broadcasted_iota(jnp.int32, (experts, META), 0)

    owner = (lane // TILE) % PLANE
    at = (lane // STRIP) * TILE + lane % TILE
    first = LATE * TILE
    spare = first - CAP
    own_at = jnp.where(at < first, at + TILE, at - first)
    far_at = jnp.where(at < first, at - spare, -1)
    token = lax.broadcasted_iota(jnp.int32, (tokens, META), 0).astype(f32) + 1.0
    z = lax.axis_index("sp_0")
    meta[...] = jnp.zeros_like(meta)
    for by in range(Z):
        side = 1 if by >= GROUPS else 0
        held = (far_at if side else own_at) if by % GROUPS == 0 else at - side * CAP
        within = held[0:1].astype(f32)
        spread = jnp.where(expert - owner == lax.rem(z + by, Z) * PLANE, 1.0, 0.0).astype(bf16)
        put = jnp.dot(place, spread, preferred_element_type=f32) == within
        tags = jnp.where(put, token + side * tokens, 0.0)
        weights = jnp.dot(high, spread, preferred_element_type=f32) + jnp.dot(
            low, spread, preferred_element_type=f32
        )
        meta[by, 0:1] = jnp.sum(tags, axis=0, keepdims=True)
        meta[by, 1:2] = jnp.sum(jnp.where(put, weights, 0.0), axis=0, keepdims=True)


def layer_kernel(
    taps,
    mix_gain,
    pre_gain,
    post_gain,
    routes,
    route_weights,
    x_hbm,
    gb_hbm,
    gc_hbm,
    proj_hbm,
    resid_hbm,
    wg_hbm,
    wu_hbm,
    wd_hbm,
    sg_hbm,
    su_hbm,
    sd_hbm,
    out,
    x_in,
    gb,
    gc,
    edge,
    mixed,
    conv,
    conv_in,
    proj,
    resid,
    normed,
    ag,
    meta,
    tables,
    xs,
    xr,
    fo,
    rr,
    part,
    far,
    rs,
    rv,
    acc,
    wg,
    wu,
    wd,
    sg,
    su,
    sd,
    load_sem,
    local_sem,
    edge_s,
    edge_r,
    conv_s,
    conv_r,
    wy_s,
    wy_r,
    wx_s,
    wx_r,
    wc_s,
    wc_r,
    ag_s,
    ag_r,
    meta_s,
    meta_r,
    x_s,
    x_r,
    e_s,
    e_r,
    b_s,
    b_r,
    l_s,
    l_r,
    h_s,
    h_r,
    rs_s,
    rs_r,
):
    z, x, c, y = (lax.axis_index(a) for a in SP_TP)
    me8 = x * C + c
    sp = z * PLANE + me8
    tokens, width = normed.shape
    half = width // 2

    def z_peer(by):
        return (lax.rem(z + by + Z, Z), x, c, y)

    def y_peer(by):
        return (z, x, c, lax.rem(y + by + Y, Y))

    def plane_peer(j):
        e = lax.rem(me8 + j, PLANE)
        return e, (z, e // C, lax.rem(e, C), y)

    def sp_peer(by):
        to = lax.rem(sp + by + Z * PLANE, Z * PLANE)
        return (to // PLANE, lax.rem(to, PLANE) // C, lax.rem(to, C), y)

    ahead = (z_peer(1), z_peer(-1))
    partner = (z, x, 1 - c, y)
    beside = ((z, lax.rem(x + 1, X), c, y), (z, lax.rem(x + X - 1, X), c, y))

    pairs = (
        (x_hbm, x_in),
        (gc_hbm, gc),
        (proj_hbm, proj.at[0]),
        (gb_hbm, gb),
        (resid_hbm, resid),
        (sg_hbm, sg),
        (su_hbm, su),
        (sd_hbm, sd),
        (wg_hbm, wg),
        (wu_hbm, wu),
        (wd_hbm, wd),
    )
    loads = [
        pltpu.make_async_copy(src, dst, load_sem.at[i]) for i, (src, dst) in enumerate(pairs)
    ]
    for load in loads:
        load.start()

    barrier = pltpu.get_barrier_semaphore()
    greeted = [z_peer(by) for by in range(1, Z)]
    greeted += [plane_peer(j)[1] for j in range(1, PLANE)]
    greeted += [y_peer(by) for by in range(1, Y)]
    greeted += [sp_peer(1), sp_peer(-1)]
    for device in greeted:
        pl.semaphore_signal(barrier, inc=1, device_id=device, device_id_type=MESH)
    pl.semaphore_wait(barrier, len(greeted))

    def remote(src, dst, send, recv, device):
        return pltpu.make_async_remote_copy(
            src_ref=src,
            dst_ref=dst,
            send_sem=send,
            recv_sem=recv,
            device_id=device,
            device_id_type=MESH,
        )

    started = []

    def begin(copy):
        copy.start()
        started.append(copy)
        return copy

    count, channels = x_in.shape
    loads[0].wait()
    loads[1].wait()
    edges = [
        begin(
            remote(
                ref.at[pl.ds(count - 8, 8)], edge.at[i], edge_s.at[i], edge_r.at[i], sp_peer(1)
            )
        )
        for i, ref in enumerate((x_in, gc))
    ]

    unit = proj.shape[1] // 8
    parity = lax.rem(x, 2)

    def unit_rows(core, par, sub):
        return pl.ds(pl.multiple_of((core * 4 + par * 2 + sub) * unit, unit), unit)

    def y_unit(source, by, sub):
        way = 1 if (by == 1 or (by == 2 and sub == 0)) else -1
        rows_at = unit_rows(c, parity, sub)
        return remote(
            proj.at[source, rows_at],
            proj.at[by, rows_at],
            wy_s.at[by, sub],
            wy_r.at[by, sub],
            y_peer(way),
        )

    loads[2].wait()
    units = {}
    for by, sub in ((1, 0), (3, 1), (1, 1), (3, 0)):
        units[by, sub] = begin(y_unit(0, by, sub))

    loads[3].wait()
    mixed[8 : 8 + count] = gc[...].astype(jnp.float32) * x_in[...].astype(jnp.float32)
    for copy in edges:
        copy.wait_recv()
    before = edge[1].astype(jnp.float32) * edge[0].astype(jnp.float32)
    mixed[0:8] = jnp.where(sp > 0, before, 0.0)
    reach = taps.shape[0] - 1
    tap = taps[...].astype(jnp.float32)
    convolved = tap[0:1] * mixed[8 - reach : 8 - reach + count]
    for index in range(1, reach + 1):
        at = 8 - reach + index
        convolved = convolved + tap[index : index + 1] * mixed[at : at + count]
    conv[...] = (gb[...].astype(jnp.float32) * convolved).astype(jnp.bfloat16)

    def token_rows(owner):
        return pl.ds(pl.multiple_of(owner * tokens, tokens), tokens)

    fill_tables(meta, routes, route_weights)

    def table_copy(by):
        group = by if by < GROUPS else (Z - by) % GROUPS
        slot = group * SIDE + (1 if by >= GROUPS else 0)
        return remote(meta.at[by], tables.at[slot], meta_s.at[by], meta_r.at[slot], z_peer(by))

    table_copies = [table_copy(by) for by in range(1, Z)]
    for copy in table_copies:
        copy.start()
    own_table = pltpu.make_async_copy(meta.at[0], tables.at[0], local_sem.at[1])
    own_table.start()

    def x_unit(by, sub):
        rows_at = unit_rows(c, parity, sub)
        return remote(
            proj.at[by, rows_at],
            proj.at[by, rows_at],
            wx_s.at[by, sub],
            wx_r.at[by, sub],
            beside[sub],
        )

    def core_unit(by, kind, sub):
        rows_at = unit_rows(c, parity if kind == 0 else 1 - parity, sub)
        return remote(
            proj.at[by, rows_at],
            proj.at[by, rows_at],
            wc_s.at[by, kind, sub],
            wc_r.at[by, kind, sub],
            partner,
        )

    def conv_copy(by):
        return remote(
            conv.at[token_rows(lax.rem(y + by, Y))],
            conv_in.at[by],
            conv_s.at[by],
            conv_r.at[by],
            y_peer(by),
        )

    conv_copies = []
    sides, swaps = {}, []
    waiting = []

    def side_arrived(key):
        sides[key].wait_recv()
        swaps.append(begin(core_unit(key[0], 1, key[1])))

    for by, sub in ((1, 0), (3, 1), (1, 1), (3, 0), (2, 0), (2, 1)):
        units[by, sub].wait_recv()
        if (by, sub) in ((1, 0), (3, 1)):
            units[2, sub] = begin(y_unit(by, 2, sub))
            if sub == 1:
                for to in range(1, Y):
                    conv_copies.append(begin(conv_copy(to)))
        sides[by, sub] = begin(x_unit(by, sub))
        swaps.append(begin(core_unit(by, 0, sub)))
        waiting.append((by, sub))
        if len(waiting) > 2:
            side_arrived(waiting.pop(0))
    for key in waiting:
        side_arrived(key)
    part[0:tokens] = jnp.dot(
        conv[token_rows(y)], proj[0], preferred_element_type=jnp.float32
    )
    for copy in conv_copies + swaps:
        copy.wait_recv()
    projected = part[0:tokens]
    for by in range(1, Y):
        projected = projected + jnp.dot(
            conv_in[by], proj[by], preferred_element_type=jnp.float32
        )
    loads[4].wait()
    row_scale = lax.rsqrt(jnp.mean(projected * projected, axis=1, keepdims=True) + epsilon)
    resid1 = (resid[...].astype(jnp.float32) + projected * row_scale * row_of(mix_gain)).astype(
        jnp.bfloat16
    )
    resid[...] = resid1
    wide_resid = resid1.astype(jnp.float32)
    normed[...] = (
        wide_resid
        * lax.rsqrt(jnp.mean(wide_resid * wide_resid, axis=1, keepdims=True) + epsilon)
        * row_of(pre_gain)
    ).astype(jnp.bfloat16)

    def gather_copy(src, group, side, chunk, way, step):
        return remote(
            src,
            ag.at[group, pl.ds(side * tokens, tokens), pl.ds(chunk * half, half)],
            ag_s.at[way, step, chunk],
            ag_r.at[way, step, chunk],
            ahead[way],
        )

    arriving = {}
    for chunk in range(2):
        for way in range(2):
            src = normed.at[pl.ds(0, tokens), pl.ds(chunk * half, half)]
            arriving[way, chunk] = begin(gather_copy(src, 1, way, chunk, way, 0))
    own_rows = pltpu.make_async_copy(normed, ag.at[0, pl.ds(0, tokens)], local_sem.at[0])
    own_rows.start()

    def slots_copies(src, dst, group, tiles, cols, send, recv):
        def view(ref, e):
            strip = pl.ds(pl.multiple_of(e * TILE, TILE), TILE)
            return ref.at[group, pl.ds(tiles[0], tiles[1] - tiles[0]), strip, pl.ds(*cols)]

        copies = []
        for j in range(1, PLANE):
            e, device = plane_peer(j)
            copies.append(remote(view(src, e), view(dst, me8), send(j), recv(j), device))
        copies.append(pltpu.make_async_copy(view(src, me8), view(dst, me8), send(0)))
        for copy in copies:
            copy.start()
        return copies

    whole = (0, width)
    halves = ((0, half), (half, half))

    def finish(copies):
        for copy in copies:
            copy.wait()

    f32, bf16 = jnp.float32, jnp.bfloat16
    late_rows = LATE * STRIP

    own_table.wait()
    token = lax.broadcasted_iota(jnp.int32, (tokens, SLOTS - late_rows), 0).astype(f32)
    chosen = jnp.where(token + 1.0 == tables[0, 0:1, late_rows:SLOTS], 1.0, 0.0).astype(bf16)
    xs[0, LATE] = lax.dot_general(
        chosen, normed[...], (((0,), (0,)), ((), ())), preferred_element_type=f32
    ).astype(bf16)
    early = slots_copies(
        xs, xr, 0, (LATE, TILES), whole, lambda j: e_s.at[j], lambda j: e_r.at[j]
    )

    for load in loads[5:8]:
        load.wait()
    rows = normed[...]
    shared_g = jnp.dot(rows, sg[...], preferred_element_type=f32)
    shared_u = jnp.dot(rows, su[...], preferred_element_type=f32)
    shared_h = (shared_g * jax.nn.sigmoid(shared_g) * shared_u).astype(bf16)
    acc[...] = jnp.dot(shared_h, sd[...], preferred_element_type=f32)
    for load in loads[8:]:
        load.wait()
    own_rows.wait()
    finish(table_copies)

    def table(group, row, tiles):
        both = tables[2 * group] + tables[2 * group + 1]
        if tiles[0]:
            both = pltpu.roll(both, META - tiles[0] * STRIP, 1)
        return both[row : row + 1, 0 : (tiles[1] - tiles[0]) * STRIP]

    def hits(group, rows, tiles):
        first, last = rows
        shape = (last - first, (tiles[1] - tiles[0]) * STRIP)
        row = lax.broadcasted_iota(jnp.int32, shape, 0).astype(f32)
        return row + (first + 1.0) == table(group, 0, tiles)

    def dispatch(group, chunk, tiles):
        picks = jnp.where(hits(group, (0, 2 * tokens), tiles), 1.0, 0.0).astype(bf16)
        cols = slice(chunk * half, (chunk + 1) * half)
        xs[group, tiles[0] : tiles[1], :, cols] = (
            lax.dot_general(
                picks,
                ag[group, :, cols],
                (((0,), (0,)), ((), ())),
                preferred_element_type=f32,
            )
            .astype(bf16)
            .reshape(tiles[1] - tiles[0], STRIP, half)
        )
        return slots_copies(
            xs,
            xr,
            group,
            tiles,
            halves[chunk],
            lambda j: x_s.at[group, chunk, j],
            lambda j: x_r.at[group, chunk, j],
        )

    def experts(group, tiles):
        count = tiles[1] - tiles[0]
        rows_in = xr[group, tiles[0] : tiles[1]].reshape(count * STRIP, width)
        gate_h = jnp.dot(rows_in, wg[...], preferred_element_type=f32)
        up_h = jnp.dot(rows_in, wu[...], preferred_element_type=f32)
        hidden = (gate_h * jax.nn.sigmoid(gate_h) * up_h).astype(bf16)
        fo[group, tiles[0] : tiles[1]] = (
            jnp.dot(hidden, wd[...], preferred_element_type=f32)
            .astype(bf16)
            .reshape(count, STRIP, width)
        )

    def give(group, tiles):
        return slots_copies(
            fo, rr, group, tiles, whole, lambda j: b_s.at[group, j], lambda j: b_r.at[group, j]
        )

    def give_part(tiles, chunk, part_no):
        return slots_copies(
            fo,
            rr,
            GROUPS - 1,
            tiles,
            halves[chunk],
            lambda j: h_s.at[part_no, chunk, j],
            lambda j: h_r.at[part_no, chunk, j],
        )

    def combine(group, rows, tiles, cols):
        weights = jnp.where(hits(group, rows, tiles), table(group, 1, tiles), 0.0)
        high = weights.astype(bf16)
        low = (weights - high.astype(f32)).astype(bf16)
        at, size = cols
        back = rr[group, tiles[0] : tiles[1], :, at : at + size]
        back = back.reshape((tiles[1] - tiles[0]) * STRIP, size)
        return jnp.dot(high, back, preferred_element_type=f32) + jnp.dot(
            low, back, preferred_element_type=f32
        )

    every, later, side_tiles = (0, TILES), (0, LATE), ((0, 2), (1, 3))

    dealt = {}
    for step in range(1, GROUPS):
        passed = {}
        dealt[step] = []
        farthest = step == GROUPS - 1
        for chunk in range(2):
            for way in range(2):
                arriving[way, chunk].wait_recv()
                if farthest and chunk != way:
                    continue
                src = ag.at[step, pl.ds(way * tokens, tokens), pl.ds(chunk * half, half)]
                group, side = (0, 1) if farthest else (step + 1, way)
                passed[way, chunk] = begin(gather_copy(src, group, side, chunk, way, step))
            dealt[step] += dispatch(step, chunk, every)
            if chunk == 0 and step > 1:
                finish(dealt[step - 1])
                experts(step - 1, every)
        arriving = passed
    dealt[0] = []
    for chunk in range(2):
        arriving[chunk, chunk].wait_recv()
        dealt[0] += dispatch(0, chunk, later)
    last = GROUPS - 1
    finish(dealt[last])
    experts(last, every)
    given = {(last, 0): give_part(side_tiles[0], 1, 0) + give_part(side_tiles[1], 0, 0)}
    finish(dealt[0])
    experts(0, later)
    given[0] = give(0, later)
    given[last, 1] = give_part((2, 3), 1, 1) + give_part((0, 1), 0, 1)
    for group in range(last - 1, 0, -1):
        given[group] = give(group, every)
    finish(early)
    experts(0, (LATE, TILES))
    given_early = slots_copies(
        fo, rr, 0, (LATE, TILES), whole, lambda j: l_s.at[j], lambda j: l_r.at[j]
    )

    unit_cols = width // UNITS

    def send_on(side, hop, no, total):
        cols = pl.ds(no * unit_cols, unit_cols)
        rs[side, hop, :, no * unit_cols : (no + 1) * unit_cols] = total.astype(bf16)
        return begin(
            remote(
                rs.at[side, hop, pl.ds(0, tokens), cols],
                rv.at[side, hop, pl.ds(0, tokens), cols],
                rs_s.at[side, hop, no],
                rs_r.at[side, hop, no],
                ahead[1 - side],
            )
        )

    def own_term(side, no):
        return part[
            side * tokens : (side + 1) * tokens, no * unit_cols : (no + 1) * unit_cols
        ]

    def came(side, hop, no):
        return rv[side, hop, :, no * unit_cols : (no + 1) * unit_cols].astype(f32)

    def units_of(chunk):
        return range(chunk * UNITS // 2, (chunk + 1) * UNITS // 2)

    def add_on(coming, passed, hop, flip):
        for one, two in zip(units_of(flip), units_of(1 - flip)):
            for side, no in ((0, one), (1, two)):
                total = own_term(side, no)
                if (side, no) in coming:
                    coming[side, no].wait_recv()
                    total = total + came(side, hop - 1, no)
                passed[side, no] = send_on(side, hop, no, total)

    def side_rows(side):
        return (side * tokens, (side + 1) * tokens)

    coming, passed = {}, {}
    finish(given[last, 0])
    for side in range(2):
        at = (1 - side) * half
        part[side * tokens : (side + 1) * tokens, at : at + half] = combine(
            last, side_rows(side), side_tiles[side], (at, half)
        )
    add_on(coming, passed, 1, 1)
    finish(given[0])
    far[...] = combine(0, side_rows(1), later, whole)
    for one, two in zip(units_of(0), units_of(1)):
        for side, no in ((0, one), (1, two)):
            value = far[:, no * unit_cols : (no + 1) * unit_cols]
            coming[side, no] = send_on(side, 0, no, value)
    finish(given[last, 1])
    for side in range(2):
        at = side * half
        part[side * tokens : (side + 1) * tokens, at : at + half] = combine(
            last, side_rows(side), side_tiles[side], (at, half)
        )
    add_on(coming, passed, 1, 0)
    for hop in range(2, GROUPS):
        coming, passed = passed, {}
        group = GROUPS - hop
        finish(given[group])
        part[...] = combine(group, (0, 2 * tokens), every, whole)
        add_on(coming, passed, hop, 1)
        add_on(coming, passed, hop, 0)
    finish(given_early)
    acc[...] += combine(0, side_rows(0), every, whole)
    for flip in (1, 0):
        for one, two in zip(units_of(flip), units_of(1 - flip)):
            for side, no in ((0, one), (1, two)):
                passed[side, no].wait_recv()
                acc[:, no * unit_cols : (no + 1) * unit_cols] += came(side, last, no)

    branch = acc[...]
    factor = lax.rsqrt(jnp.mean(branch * branch, axis=1, keepdims=True) + epsilon)
    out[...] = (resid[...].astype(jnp.float32) + branch * factor * row_of(post_gain)).astype(
        jnp.bfloat16
    )
    for copy in started:
        copy.wait_send()


def body(
    x_in,
    gate_b,
    gate_c,
    conv_taps,
    out_proj,
    mix_gain,
    resid,
    pre_gain,
    expert_gate,
    expert_up,
    expert_down,
    shared_gate,
    shared_up,
    shared_down,
    post_gain,
    routes,
    route_weights,
):
    tokens, width = resid.shape
    rows, channels = x_in.shape
    hidden = expert_gate.shape[2]
    shared = shared_gate.shape[1]
    bf16, f32 = jnp.bfloat16, jnp.float32
    vmem = pl.BlockSpec(memory_space=pltpu.VMEM)
    hbm = pl.BlockSpec(memory_space=pl.ANY)
    dma = pltpu.SemaphoreType.DMA
    return pl.pallas_call(
        layer_kernel,
        out_shape=pltpu.VMEM((tokens, width), bf16),
        in_specs=[vmem] * 6 + [hbm] * 11,
        out_specs=vmem,
        scratch_shapes=[
            pltpu.VMEM((rows, channels), bf16),
            pltpu.VMEM((rows, channels), bf16),
            pltpu.VMEM((rows, channels), bf16),
            pltpu.VMEM((2, 8, channels), bf16),
            pltpu.VMEM((rows + 8, channels), f32),
            pltpu.VMEM((rows, channels), bf16),
            pltpu.VMEM((Y, tokens, channels), bf16),
            pltpu.VMEM((Y, channels, width), bf16),
            pltpu.VMEM((tokens, width), bf16),
            pltpu.VMEM((tokens, width), bf16),
            pltpu.VMEM((GROUPS, 2 * tokens, width), bf16),
            pltpu.VMEM((Z, 8, META), f32),
            pltpu.VMEM((Z, 8, META), f32),
            pltpu.VMEM((GROUPS, TILES, STRIP, width), bf16),
            pltpu.VMEM((GROUPS, TILES, STRIP, width), bf16),
            pltpu.VMEM((GROUPS, TILES, STRIP, width), bf16),
            pltpu.VMEM((GROUPS, TILES, STRIP, width), bf16),
            pltpu.VMEM((2 * tokens, width), f32),
            pltpu.VMEM((tokens, width), f32),
            pltpu.VMEM((2, GROUPS, tokens, width), bf16),
            pltpu.VMEM((2, GROUPS, tokens, width), bf16),
            pltpu.VMEM((tokens, width), f32),
            pltpu.VMEM((width, hidden), bf16),
            pltpu.VMEM((width, hidden), bf16),
            pltpu.VMEM((hidden, width), bf16),
            pltpu.VMEM((width, shared), bf16),
            pltpu.VMEM((width, shared), bf16),
            pltpu.VMEM((shared, width), bf16),
            dma((11,)),
            dma((2,)),
            dma((2,)),
            dma((2,)),
            dma((Y,)),
            dma((Y,)),
            dma((Y, 2)),
            dma((Y, 2)),
            dma((Y, 2)),
            dma((Y, 2)),
            dma((Y, 2, 2)),
            dma((Y, 2, 2)),
            dma((2, GROUPS, 2)),
            dma((2, GROUPS, 2)),
            dma((Z,)),
            dma((Z,)),
            dma((GROUPS, 2, PLANE)),
            dma((GROUPS, 2, PLANE)),
            dma((PLANE,)),
            dma((PLANE,)),
            dma((GROUPS, PLANE)),
            dma((GROUPS, PLANE)),
            dma((PLANE,)),
            dma((PLANE,)),
            dma((2, 2, PLANE)),
            dma((2, 2, PLANE)),
            dma((2, GROUPS, UNITS)),
            dma((2, GROUPS, UNITS)),
        ],
        compiler_params=pltpu.CompilerParams(
            collective_id=0, has_side_effects=True, vmem_limit_bytes=63 * 1024 * 1024
        ),
    )(
        conv_taps,
        mix_gain.reshape(-1, 128),
        pre_gain.reshape(-1, 128),
        post_gain.reshape(-1, 128),
        routes.T,
        route_weights.T,
        x_in,
        gate_b,
        gate_c,
        out_proj,
        resid,
        expert_gate[0],
        expert_up[0],
        expert_down[0],
        shared_gate,
        shared_up,
        shared_down,
    )


def solution(mesh):
    finer = Mesh(mesh.devices.reshape(Z, X, C, mesh.shape["tp"]), SP_TP)
    placed = (
        P(SP, "tp"),
        P(SP, "tp"),
        P(SP, "tp"),
        P(None, "tp"),
        P("tp", None),
        P(),
        P(SP_TP, None),
        P(),
        P(SP, None, None),
        P(SP, None, None),
        P(SP, None, None),
        P(),
        P(),
        P(),
        P(),
        P(SP_TP, None),
        P(SP_TP, None),
    )
    return jax.shard_map(
        body, mesh=finer, in_specs=placed, out_specs=P(SP_TP, None), check_vma=False
    )
```

profile of v0, /device:TPU:1, one launch (start us, length us, event | category | flops | bytes accessed | tf_op | source)
XLA Modules:
  0.0 134.0 jit_solution(12938994660827889563)
XLA Ops:
  0.0 133.2 %shard_map.163 = bf16[128,2048]{1,0:T(8,128)(2,1)S(1)} custom-call(bf16[3,256]{1,0:T(4,128)(2,1)} %taps.1, bf16[16,128]{1,0:T(8,128)(2,1)} %bitcast.11, bf16[16,128]{1,0:T(8,128)(2,1)} %bitcast.12, bf16[16,128]{1,0:T(8,128)(2,1)} %bitcast.13, s32[4,128]{1,0:T(4,128)} %bitcast.14, f32[4,128]{1,0:T(4,128)} %bitcast.15, bf16[512,256]{1,0:T(8,128)(2,1)} %x_hbm.1, ...), custom_call_target="tpu_custom_call" | custom-call | tf_op jit(solution)/shard_map/pallas_call | solution.py:651
  133.2 0.8 copy.19
where the time goes:
time: 134 us
  Pallas kernels  133 us (99%)
    pallas_call x1, Pallas kernels, body(): pl.pallas_call(layer_kernel, out_shape=pltpu.VMEM((tokens, width), bf16),...  133 us

commit v1 on v0

--- a/solution.py
+++ b/solution.py
@@ -24,7 +24,9 @@
 TILES = ROWS // TILE
 STRIP = PLANE * TILE
 LATE = 2
-UNITS = 4
+PARTS = 4
+HOPS = Z - 1
+SUBS = 4
 
 
 def row_of(ref):
@@ -115,7 +117,6 @@
     fo,
     rr,
     part,
-    far,
     rs,
     rv,
     acc,
@@ -159,6 +160,7 @@
     sp = z * PLANE + me8
     tokens, width = normed.shape
     half = width // 2
+    share = width // PARTS
 
     def z_peer(by):
         return (lax.rem(z + by + Z, Z), x, c, y)
@@ -176,7 +178,12 @@
 
     ahead = (z_peer(1), z_peer(-1))
     partner = (z, x, 1 - c, y)
-    beside = ((z, lax.rem(x + 1, X), c, y), (z, lax.rem(x + X - 1, X), c, y))
+    beside = (
+        (z, lax.rem(x + 1, X), c, y),
+        (z, lax.rem(x + X - 1, X), c, y),
+        z_peer(1),
+        z_peer(-1),
+    )
 
     pairs = (
         (x_hbm, x_in),
@@ -204,6 +211,7 @@
     greeted += [sp_peer(1), sp_peer(-1)]
     for device in greeted:
         pl.semaphore_signal(barrier, inc=1, device_id=device, device_id_type=MESH)
+    fill_tables(meta, routes, route_weights)
     pl.semaphore_wait(barrier, len(greeted))
 
     def remote(src, dst, send, recv, device):
@@ -235,14 +243,14 @@
         for i, ref in enumerate((x_in, gc))
     ]
 
-    unit = proj.shape[1] // 8
-    parity = lax.rem(x, 2)
+    unit = proj.shape[1] // (2 * C * SUBS)
+    parity = lax.rem(x + z, 2)
 
     def unit_rows(core, par, sub):
-        return pl.ds(pl.multiple_of((core * 4 + par * 2 + sub) * unit, unit), unit)
+        return pl.ds(pl.multiple_of(((core * 2 + par) * SUBS + sub) * unit, unit), unit)
 
     def y_unit(source, by, sub):
-        way = 1 if (by == 1 or (by == 2 and sub == 0)) else -1
+        way = 1 if (by == 1 or (by == 2 and sub < SUBS // 2)) else -1
         rows_at = unit_rows(c, parity, sub)
         return remote(
             proj.at[source, rows_at],
@@ -254,27 +262,28 @@
 
     loads[2].wait()
     units = {}
-    for by, sub in ((1, 0), (3, 1), (1, 1), (3, 0)):
+    near = [(by, (sub + (0 if by == 1 else 2)) % SUBS) for sub in range(SUBS) for by in (1, 3)]
+    for by, sub in near:
         units[by, sub] = begin(y_unit(0, by, sub))
 
     loads[3].wait()
     mixed[8 : 8 + count] = gc[...].astype(jnp.float32) * x_in[...].astype(jnp.float32)
-    for copy in edges:
-        copy.wait_recv()
-    before = edge[1].astype(jnp.float32) * edge[0].astype(jnp.float32)
-    mixed[0:8] = jnp.where(sp > 0, before, 0.0)
     reach = taps.shape[0] - 1
     tap = taps[...].astype(jnp.float32)
-    convolved = tap[0:1] * mixed[8 - reach : 8 - reach + count]
-    for index in range(1, reach + 1):
-        at = 8 - reach + index
-        convolved = convolved + tap[index : index + 1] * mixed[at : at + count]
-    conv[...] = (gb[...].astype(jnp.float32) * convolved).astype(jnp.bfloat16)
+    mixed[0:8] = jnp.zeros((8, channels), jnp.float32)
+
+    def convolve(first, last):
+        total = None
+        for index in range(reach + 1):
+            at = 8 - reach + index
+            term = tap[index : index + 1] * mixed[at + first : at + last]
+            total = term if total is None else total + term
+        conv[first:last] = (gb[first:last].astype(jnp.float32) * total).astype(jnp.bfloat16)
+
+    convolve(0, count)
 
     def token_rows(owner):
         return pl.ds(pl.multiple_of(owner * tokens, tokens), tokens)
-
-    fill_tables(meta, routes, route_weights)
 
     def table_copy(by):
         group = by if by < GROUPS else (Z - by) % GROUPS
@@ -317,37 +326,41 @@
         )
 
     conv_copies = []
-    sides, swaps = {}, []
+    sides, swaps = {}, {}
     waiting = []
 
-    def side_arrived(key):
-        sides[key].wait_recv()
-        swaps.append(begin(core_unit(key[0], 1, key[1])))
-
-    for by, sub in ((1, 0), (3, 1), (1, 1), (3, 0), (2, 0), (2, 1)):
+    def side_arrived(by, sub):
+        sides[by, sub].wait_recv()
+        swaps[by, 1, sub] = begin(core_unit(by, 1, sub))
+
+    relayed = {(1, 0), (1, 1), (3, 2), (3, 3)}
+    for by, sub in near + [(2, 0), (2, 2), (2, 1), (2, 3)]:
         units[by, sub].wait_recv()
-        if (by, sub) in ((1, 0), (3, 1)):
+        if (by, sub) in relayed:
             units[2, sub] = begin(y_unit(by, 2, sub))
-            if sub == 1:
-                for to in range(1, Y):
-                    conv_copies.append(begin(conv_copy(to)))
         sides[by, sub] = begin(x_unit(by, sub))
-        swaps.append(begin(core_unit(by, 0, sub)))
+        swaps[by, 0, sub] = begin(core_unit(by, 0, sub))
         waiting.append((by, sub))
-        if len(waiting) > 2:
-            side_arrived(waiting.pop(0))
-    for key in waiting:
-        side_arrived(key)
-    part[0:tokens] = jnp.dot(
-        conv[token_rows(y)], proj[0], preferred_element_type=jnp.float32
-    )
-    for copy in conv_copies + swaps:
-        copy.wait_recv()
+        if (by, sub) == (3, 3):
+            for copy in edges:
+                copy.wait_recv()
+            before = edge[1].astype(jnp.float32) * edge[0].astype(jnp.float32)
+            mixed[0:8] = jnp.where(sp > 0, before, 0.0)
+            convolve(0, 8)
+            for to in range(1, Y):
+                conv_copies.append(begin(conv_copy(to)))
+        if len(waiting) > 4:
+            side_arrived(*waiting.pop(0))
+    part[0:tokens] = jnp.dot(conv[token_rows(y)], proj[0], preferred_element_type=jnp.float32)
+    for by, sub in waiting:
+        side_arrived(by, sub)
+    for by in (1, 3, 2):
+        conv_copies[by - 1].wait_recv()
+        for kind in range(2):
+            for sub in range(SUBS):
+                swaps[by, kind, sub].wait_recv()
+        part[0:tokens] += jnp.dot(conv_in[by], proj[by], preferred_element_type=jnp.float32)
     projected = part[0:tokens]
-    for by in range(1, Y):
-        projected = projected + jnp.dot(
-            conv_in[by], proj[by], preferred_element_type=jnp.float32
-        )
     loads[4].wait()
     row_scale = lax.rsqrt(jnp.mean(projected * projected, axis=1, keepdims=True) + epsilon)
     resid1 = (resid[...].astype(jnp.float32) + projected * row_scale * row_of(mix_gain)).astype(
@@ -364,16 +377,16 @@
     def gather_copy(src, group, side, chunk, way, step):
         return remote(
             src,
-            ag.at[group, pl.ds(side * tokens, tokens), pl.ds(chunk * half, half)],
+            ag.at[group, pl.ds(side * tokens, tokens), pl.ds(chunk * share, share)],
             ag_s.at[way, step, chunk],
             ag_r.at[way, step, chunk],
             ahead[way],
         )
 
     arriving = {}
-    for chunk in range(2):
+    for chunk in range(PARTS):
         for way in range(2):
-            src = normed.at[pl.ds(0, tokens), pl.ds(chunk * half, half)]
+            src = normed.at[pl.ds(0, tokens), pl.ds(chunk * share, share)]
             arriving[way, chunk] = begin(gather_copy(src, 1, way, chunk, way, 0))
     own_rows = pltpu.make_async_copy(normed, ag.at[0, pl.ds(0, tokens)], local_sem.at[0])
     own_rows.start()
@@ -438,7 +451,7 @@
 
     def dispatch(group, chunk, tiles):
         picks = jnp.where(hits(group, (0, 2 * tokens), tiles), 1.0, 0.0).astype(bf16)
-        cols = slice(chunk * half, (chunk + 1) * half)
+        cols = slice(chunk * share, (chunk + 1) * share)
         xs[group, tiles[0] : tiles[1], :, cols] = (
             lax.dot_general(
                 picks,
@@ -447,14 +460,14 @@
                 preferred_element_type=f32,
             )
             .astype(bf16)
-            .reshape(tiles[1] - tiles[0], STRIP, half)
+            .reshape(tiles[1] - tiles[0], STRIP, share)
         )
         return slots_copies(
             xs,
             xr,
             group,
             tiles,
-            halves[chunk],
+            (chunk * share, share),
             lambda j: x_s.at[group, chunk, j],
             lambda j: x_r.at[group, chunk, j],
         )
@@ -471,20 +484,15 @@
             .reshape(count, STRIP, width)
         )
 
-    def give(group, tiles):
-        return slots_copies(
-            fo, rr, group, tiles, whole, lambda j: b_s.at[group, j], lambda j: b_r.at[group, j]
-        )
-
-    def give_part(tiles, chunk, part_no):
+    def give_part(group, tiles, chunk, no):
         return slots_copies(
             fo,
             rr,
-            GROUPS - 1,
+            group,
             tiles,
             halves[chunk],
-            lambda j: h_s.at[part_no, chunk, j],
-            lambda j: h_r.at[part_no, chunk, j],
+            lambda j: h_s.at[group, no, chunk, j],
+            lambda j: h_r.at[group, no, chunk, j],
         )
 
     def combine(group, rows, tiles, cols):
@@ -500,117 +508,110 @@
 
     every, later, side_tiles = (0, TILES), (0, LATE), ((0, 2), (1, 3))
 
-    dealt = {}
+    def reduced_copy(way, hop, no):
+        cols = pl.ds(no * share, share)
+        return remote(
+            rs.at[way, hop, pl.ds(0, tokens), cols],
+            rv.at[way, hop, pl.ds(0, tokens), cols],
+            rs_s.at[way, hop, no],
+            rs_r.at[way, hop, no],
+            ahead[way],
+        )
+
+    def side_rows(side):
+        return (side * tokens, (side + 1) * tokens)
+
+    def own_term(way, hop):
+        distance = hop + 1
+        cols = halves[way]
+        if distance == GROUPS:
+            return combine(0, side_rows(1), later, cols)
+        if distance < GROUPS:
+            group, side = distance, way
+        else:
+            group, side = Z - distance, 1 - way
+        return combine(group, side_rows(side), side_tiles[side], cols)
+
+    def came(way, hop, no):
+        return rv[way, hop, :, no * share : (no + 1) * share].astype(f32)
+
+    def reduce_step(hop, coming):
+        terms = [own_term(way, hop) for way in range(2)]
+        passed = {}
+        for no in range(2):
+            for way in range(2):
+                total = terms[way][:, no * share : (no + 1) * share]
+                if hop:
+                    coming[way, no].wait_recv()
+                    total = total + came(way, hop - 1, no)
+                rs[way, hop, :, no * share : (no + 1) * share] = total.astype(bf16)
+                passed[way, no] = begin(reduced_copy(way, hop, no))
+        return passed
+
+    def give_first(group):
+        return give_part(group, side_tiles[0], 0, 0) + give_part(group, side_tiles[1], 1, 0)
+
+    def give_rest(group):
+        return give_part(group, (2, 3), 0, 1) + give_part(group, (0, 1), 1, 1)
+
+    dealt, given, rest = {}, {}, {}
     for step in range(1, GROUPS):
         passed = {}
         dealt[step] = []
         farthest = step == GROUPS - 1
-        for chunk in range(2):
+        for chunk in range(PARTS):
             for way in range(2):
                 arriving[way, chunk].wait_recv()
-                if farthest and chunk != way:
+                if farthest and chunk % 2 != way:
                     continue
-                src = ag.at[step, pl.ds(way * tokens, tokens), pl.ds(chunk * half, half)]
+                src = ag.at[step, pl.ds(way * tokens, tokens), pl.ds(chunk * share, share)]
                 group, side = (0, 1) if farthest else (step + 1, way)
                 passed[way, chunk] = begin(gather_copy(src, group, side, chunk, way, step))
             dealt[step] += dispatch(step, chunk, every)
-            if chunk == 0 and step > 1:
+            if chunk == 1 and step > 1:
                 finish(dealt[step - 1])
                 experts(step - 1, every)
+                given[step - 1] = give_first(step - 1)
+            if chunk == PARTS - 1 and step == 1:
+                finish(early)
+                experts(0, (LATE, TILES))
         arriving = passed
+    finish(given[1])
+    coming = reduce_step(0, {})
     dealt[0] = []
-    for chunk in range(2):
-        arriving[chunk, chunk].wait_recv()
+    for chunk in range(PARTS):
+        arriving[chunk % 2, chunk].wait_recv()
         dealt[0] += dispatch(0, chunk, later)
     last = GROUPS - 1
     finish(dealt[last])
     experts(last, every)
-    given = {(last, 0): give_part(side_tiles[0], 1, 0) + give_part(side_tiles[1], 0, 0)}
+    given[last] = give_first(last)
+    finish(given[2])
+    coming = reduce_step(1, coming)
     finish(dealt[0])
     experts(0, later)
-    given[0] = give(0, later)
-    given[last, 1] = give_part((2, 3), 1, 1) + give_part((0, 1), 0, 1)
-    for group in range(last - 1, 0, -1):
-        given[group] = give(group, every)
-    finish(early)
-    experts(0, (LATE, TILES))
+    given[0] = slots_copies(
+        fo, rr, 0, later, whole, lambda j: b_s.at[j], lambda j: b_r.at[j]
+    )
+    for group in range(last, 0, -1):
+        rest[group] = give_rest(group)
     given_early = slots_copies(
         fo, rr, 0, (LATE, TILES), whole, lambda j: l_s.at[j], lambda j: l_r.at[j]
     )
-
-    unit_cols = width // UNITS
-
-    def send_on(side, hop, no, total):
-        cols = pl.ds(no * unit_cols, unit_cols)
-        rs[side, hop, :, no * unit_cols : (no + 1) * unit_cols] = total.astype(bf16)
-        return begin(
-            remote(
-                rs.at[side, hop, pl.ds(0, tokens), cols],
-                rv.at[side, hop, pl.ds(0, tokens), cols],
-                rs_s.at[side, hop, no],
-                rs_r.at[side, hop, no],
-                ahead[1 - side],
-            )
-        )
-
-    def own_term(side, no):
-        return part[
-            side * tokens : (side + 1) * tokens, no * unit_cols : (no + 1) * unit_cols
-        ]
-
-    def came(side, hop, no):
-        return rv[side, hop, :, no * unit_cols : (no + 1) * unit_cols].astype(f32)
-
-    def units_of(chunk):
-        return range(chunk * UNITS // 2, (chunk + 1) * UNITS // 2)
-
-    def add_on(coming, passed, hop, flip):
-        for one, two in zip(units_of(flip), units_of(1 - flip)):
-            for side, no in ((0, one), (1, two)):
-                total = own_term(side, no)
-                if (side, no) in coming:
-                    coming[side, no].wait_recv()
-                    total = total + came(side, hop - 1, no)
-                passed[side, no] = send_on(side, hop, no, total)
-
-    def side_rows(side):
-        return (side * tokens, (side + 1) * tokens)
-
-    coming, passed = {}, {}
-    finish(given[last, 0])
-    for side in range(2):
-        at = (1 - side) * half
-        part[side * tokens : (side + 1) * tokens, at : at + half] = combine(
-            last, side_rows(side), side_tiles[side], (at, half)
-        )
-    add_on(coming, passed, 1, 1)
+    finish(given[last])
+    coming = reduce_step(2, coming)
     finish(given[0])
-    far[...] = combine(0, side_rows(1), later, whole)
-    for one, two in zip(units_of(0), units_of(1)):
-        for side, no in ((0, one), (1, two)):
-            value = far[:, no * unit_cols : (no + 1) * unit_cols]
-            coming[side, no] = send_on(side, 0, no, value)
-    finish(given[last, 1])
-    for side in range(2):
-        at = side * half
-        part[side * tokens : (side + 1) * tokens, at : at + half] = combine(
-            last, side_rows(side), side_tiles[side], (at, half)
-        )
-    add_on(coming, passed, 1, 0)
-    for hop in range(2, GROUPS):
-        coming, passed = passed, {}
-        group = GROUPS - hop
-        finish(given[group])
-        part[...] = combine(group, (0, 2 * tokens), every, whole)
-        add_on(coming, passed, hop, 1)
-        add_on(coming, passed, hop, 0)
+    coming = reduce_step(3, coming)
+    for hop in range(GROUPS, HOPS):
+        finish(rest[HOPS - hop])
+        coming = reduce_step(hop, coming)
     finish(given_early)
     acc[...] += combine(0, side_rows(0), every, whole)
-    for flip in (1, 0):
-        for one, two in zip(units_of(flip), units_of(1 - flip)):
-            for side, no in ((0, one), (1, two)):
-                passed[side, no].wait_recv()
-                acc[:, no * unit_cols : (no + 1) * unit_cols] += came(side, last, no)
+    for no in range(2):
+        for way in range(2):
+            coming[way, no].wait_recv()
+            at = way * half + no * share
+            acc[:, at : at + share] += came(way, HOPS - 1, no)
 
     branch = acc[...]
     factor = lax.rsqrt(jnp.mean(branch * branch, axis=1, keepdims=True) + epsilon)
@@ -671,10 +672,9 @@
             pltpu.VMEM((GROUPS, TILES, STRIP, width), bf16),
             pltpu.VMEM((GROUPS, TILES, STRIP, width), bf16),
             pltpu.VMEM((GROUPS, TILES, STRIP, width), bf16),
-            pltpu.VMEM((2 * tokens, width), f32),
             pltpu.VMEM((tokens, width), f32),
-            pltpu.VMEM((2, GROUPS, tokens, width), bf16),
-            pltpu.VMEM((2, GROUPS, tokens, width), bf16),
+            pltpu.VMEM((2, HOPS, tokens, width // 2), bf16),
+            pltpu.VMEM((2, HOPS, tokens, width // 2), bf16),
             pltpu.VMEM((tokens, width), f32),
             pltpu.VMEM((width, hidden), bf16),
             pltpu.VMEM((width, hidden), bf16),
@@ -688,28 +688,28 @@
             dma((2,)),
             dma((Y,)),
             dma((Y,)),
-            dma((Y, 2)),
-            dma((Y, 2)),
-            dma((Y, 2)),
-            dma((Y, 2)),
-            dma((Y, 2, 2)),
-            dma((Y, 2, 2)),
-            dma((2, GROUPS, 2)),
-            dma((2, GROUPS, 2)),
+            dma((Y, SUBS)),
+            dma((Y, SUBS)),
+            dma((Y, SUBS)),
+            dma((Y, SUBS)),
+            dma((Y, 2, SUBS)),
+            dma((Y, 2, SUBS)),
+            dma((2, GROUPS, PARTS)),
+            dma((2, GROUPS, PARTS)),
             dma((Z,)),
             dma((Z,)),
-            dma((GROUPS, 2, PLANE)),
-            dma((GROUPS, 2, PLANE)),
+            dma((GROUPS, PARTS, PLANE)),
+            dma((GROUPS, PARTS, PLANE)),
             dma((PLANE,)),
             dma((PLANE,)),
-            dma((GROUPS, PLANE)),
-            dma((GROUPS, PLANE)),
             dma((PLANE,)),
             dma((PLANE,)),
-            dma((2, 2, PLANE)),
-            dma((2, 2, PLANE)),
-            dma((2, GROUPS, UNITS)),
-            dma((2, GROUPS, UNITS)),
+            dma((PLANE,)),
+            dma((PLANE,)),
+            dma((GROUPS, 2, 2, PLANE)),
+            dma((GROUPS, 2, 2, PLANE)),
+            dma((2, HOPS, 2)),
+            dma((2, HOPS, 2)),
         ],
         compiler_params=pltpu.CompilerParams(
             collective_id=0, has_side_effects=True, vmem_limit_bytes=63 * 1024 * 1024

time: 134 us -> 129 us (0.963)
  Pallas kernels: 133 us -> 129 us
    pallas_call x1, Pallas kernels: 133 us -> 129 us  [body(): pl.pallas_call(layer_kernel, out_shape=pltpu.VMEM((tokens, width), bf16),...]
where the time goes in v1:
time: 129 us
  Pallas kernels  129 us (100%)
    pallas_call x1, Pallas kernels, body(): pl.pallas_call(layer_kernel, out_shape=pltpu.VMEM((tokens, width), bf16),...  129 us

profile of v1, /device:TPU:1, one launch (start us, length us, event | category | flops | bytes accessed | tf_op | source)
XLA Modules:
  0.0 129.4 jit_solution(11987855449664944770)
XLA Ops:
  0.0 128.6 %shard_map.163 = bf16[128,2048]{1,0:T(8,128)(2,1)S(1)} custom-call(bf16[3,256]{1,0:T(4,128)(2,1)} %taps.1, bf16[16,128]{1,0:T(8,128)(2,1)} %bitcast.11, bf16[16,128]{1,0:T(8,128)(2,1)} %bitcast.12, bf16[16,128]{1,0:T(8,128)(2,1)} %bitcast.13, s32[4,128]{1,0:T(4,128)} %bitcast.14, f32[4,128]{1,0:T(4,128)} %bitcast.15, bf16[512,256]{1,0:T(8,128)(2,1)} %x_hbm.1, ...), custom_call_target="tpu_custom_call" | custom-call | tf_op jit(solution)/shard_map/pallas_call | solution.py:652
  128.6 0.8 copy.19

commit v2 on v1

--- a/solution.py
+++ b/solution.py
@@ -391,10 +391,14 @@
     own_rows = pltpu.make_async_copy(normed, ag.at[0, pl.ds(0, tokens)], local_sem.at[0])
     own_rows.start()
 
+    def aligned(at):
+        return at if isinstance(at, int) else pl.multiple_of(at, share)
+
     def slots_copies(src, dst, group, tiles, cols, send, recv):
         def view(ref, e):
             strip = pl.ds(pl.multiple_of(e * TILE, TILE), TILE)
-            return ref.at[group, pl.ds(tiles[0], tiles[1] - tiles[0]), strip, pl.ds(*cols)]
+            lanes = pl.ds(aligned(cols[0]), cols[1])
+            return ref.at[group, pl.ds(tiles[0], tiles[1] - tiles[0]), strip, lanes]
 
         copies = []
         for j in range(1, PLANE):
@@ -406,7 +410,6 @@
         return copies
 
     whole = (0, width)
-    halves = ((0, half), (half, half))
 
     def finish(copies):
         for copy in copies:
@@ -484,15 +487,15 @@
             .reshape(count, STRIP, width)
         )
 
-    def give_part(group, tiles, chunk, no):
+    def give_part(group, tiles, cols, turn, no):
         return slots_copies(
             fo,
             rr,
             group,
             tiles,
-            halves[chunk],
-            lambda j: h_s.at[group, no, chunk, j],
-            lambda j: h_r.at[group, no, chunk, j],
+            cols,
+            lambda j: h_s.at[group, turn, no, j],
+            lambda j: h_r.at[group, turn, no, j],
         )
 
     def combine(group, rows, tiles, cols):
@@ -500,13 +503,17 @@
         high = weights.astype(bf16)
         low = (weights - high.astype(f32)).astype(bf16)
         at, size = cols
-        back = rr[group, tiles[0] : tiles[1], :, at : at + size]
+        back = rr[group, tiles[0] : tiles[1], :, pl.ds(aligned(at), size)]
         back = back.reshape((tiles[1] - tiles[0]) * STRIP, size)
         return jnp.dot(high, back, preferred_element_type=f32) + jnp.dot(
             low, back, preferred_element_type=f32
         )
 
     every, later, side_tiles = (0, TILES), (0, LATE), ((0, 2), (1, 3))
+
+    def half_of(way, by):
+        turned = (lax.rem(z + by + Z, Z) // 2) % 2
+        return (turned if way == 0 else 1 - turned) * half
 
     def reduced_copy(way, hop, no):
         cols = pl.ds(no * share, share)
@@ -521,9 +528,10 @@
     def side_rows(side):
         return (side * tokens, (side + 1) * tokens)
 
-    def own_term(way, hop):
+    def own_term(way, hop, no):
         distance = hop + 1
-        cols = halves[way]
+        owner = distance if way else -distance
+        cols = (half_of(way, owner) + no * share, share)
         if distance == GROUPS:
             return combine(0, side_rows(1), later, cols)
         if distance < GROUPS:
@@ -535,12 +543,12 @@
     def came(way, hop, no):
         return rv[way, hop, :, no * share : (no + 1) * share].astype(f32)
 
-    def reduce_step(hop, coming):
-        terms = [own_term(way, hop) for way in range(2)]
+    def reduce_step(hop, coming, ready):
         passed = {}
         for no in range(2):
+            finish(ready[no])
             for way in range(2):
-                total = terms[way][:, no * share : (no + 1) * share]
+                total = own_term(way, hop, no)
                 if hop:
                     coming[way, no].wait_recv()
                     total = total + came(way, hop - 1, no)
@@ -549,10 +557,41 @@
         return passed
 
     def give_first(group):
-        return give_part(group, side_tiles[0], 0, 0) + give_part(group, side_tiles[1], 1, 0)
+        left = half_of(0, -group)
+        copies = []
+        for no in range(2):
+            cols = (left + no * share, share)
+            if group % 2:
+                copies.append(give_part(group, every, cols, no, 0))
+            else:
+                other = (half - left + no * share, share)
+                copies.append(
+                    give_part(group, side_tiles[0], cols, no, 0)
+                    + give_part(group, side_tiles[1], other, no, 1)
+                )
+        return copies
 
     def give_rest(group):
-        return give_part(group, (2, 3), 0, 1) + give_part(group, (0, 1), 1, 1)
+        left = half_of(0, -group)
+        if group % 2:
+            return give_part(group, every, (half - left, half), 2, 0)
+        return give_part(group, (2, 3), (left, half), 2, 0) + give_part(
+            group, (0, 1), (half - left, half), 2, 1
+        )
+
+    def give_late(no):
+        copies = []
+        for side in range(2):
+            copies += slots_copies(
+                fo,
+                rr,
+                0,
+                later,
+                (side * half + no * share, share),
+                lambda j: b_s.at[no, side, j],
+                lambda j: b_r.at[no, side, j],
+            )
+        return copies
 
     dealt, given, rest = {}, {}, {}
     for step in range(1, GROUPS):
@@ -568,7 +607,7 @@
                 group, side = (0, 1) if farthest else (step + 1, way)
                 passed[way, chunk] = begin(gather_copy(src, group, side, chunk, way, step))
             dealt[step] += dispatch(step, chunk, every)
-            if chunk == 1 and step > 1:
+            if chunk == step - 1 and step > 1:
                 finish(dealt[step - 1])
                 experts(step - 1, every)
                 given[step - 1] = give_first(step - 1)
@@ -576,8 +615,7 @@
                 finish(early)
                 experts(0, (LATE, TILES))
         arriving = passed
-    finish(given[1])
-    coming = reduce_step(0, {})
+    coming = reduce_step(0, {}, given[1])
     dealt[0] = []
     for chunk in range(PARTS):
         arriving[chunk % 2, chunk].wait_recv()
@@ -586,32 +624,26 @@
     finish(dealt[last])
     experts(last, every)
     given[last] = give_first(last)
-    finish(given[2])
-    coming = reduce_step(1, coming)
+    coming = reduce_step(1, coming, given[2])
     finish(dealt[0])
     experts(0, later)
-    given[0] = slots_copies(
-        fo, rr, 0, later, whole, lambda j: b_s.at[j], lambda j: b_r.at[j]
-    )
+    given[0] = [give_late(no) for no in range(2)]
     for group in range(last, 0, -1):
         rest[group] = give_rest(group)
     given_early = slots_copies(
         fo, rr, 0, (LATE, TILES), whole, lambda j: l_s.at[j], lambda j: l_r.at[j]
     )
-    finish(given[last])
-    coming = reduce_step(2, coming)
-    finish(given[0])
-    coming = reduce_step(3, coming)
+    coming = reduce_step(2, coming, given[last])
+    coming = reduce_step(3, coming, given[0])
     for hop in range(GROUPS, HOPS):
-        finish(rest[HOPS - hop])
-        coming = reduce_step(hop, coming)
+        coming = reduce_step(hop, coming, (rest[HOPS - hop], ()))
     finish(given_early)
     acc[...] += combine(0, side_rows(0), every, whole)
     for no in range(2):
         for way in range(2):
             coming[way, no].wait_recv()
-            at = way * half + no * share
-            acc[:, at : at + share] += came(way, HOPS - 1, no)
+            cols = pl.ds(aligned(half_of(way, 0) + no * share), share)
+            acc[:, cols] += came(way, HOPS - 1, no)
 
     branch = acc[...]
     factor = lax.rsqrt(jnp.mean(branch * branch, axis=1, keepdims=True) + epsilon)
@@ -702,12 +734,12 @@
             dma((GROUPS, PARTS, PLANE)),
             dma((PLANE,)),
             dma((PLANE,)),
+            dma((2, 2, PLANE)),
+            dma((2, 2, PLANE)),
             dma((PLANE,)),
             dma((PLANE,)),
-            dma((PLANE,)),
-            dma((PLANE,)),
-            dma((GROUPS, 2, 2, PLANE)),
-            dma((GROUPS, 2, 2, PLANE)),
+            dma((GROUPS, 3, 2, PLANE)),
+            dma((GROUPS, 3, 2, PLANE)),
             dma((2, HOPS, 2)),
             dma((2, HOPS, 2)),
         ],

time: 129 us -> 126 us (0.977)
  Pallas kernels: 129 us -> 125 us
    pallas_call x1, Pallas kernels: 129 us -> 125 us  [body(): pl.pallas_call(layer_kernel, out_shape=pltpu.VMEM((tokens, width), bf16),...]
where the time goes in v2:
time: 126 us
  Pallas kernels  125 us (99%)
    pallas_call x1, Pallas kernels, body(): pl.pallas_call(layer_kernel, out_shape=pltpu.VMEM((tokens, width), bf16),...  125 us

profile of v2, /device:TPU:1, one launch (start us, length us, event | category | flops | bytes accessed | tf_op | source)
XLA Modules:
  0.0 126.0 jit_solution(3249330125582559683)
XLA Ops:
  0.0 125.1 %shard_map.163 = bf16[128,2048]{1,0:T(8,128)(2,1)S(1)} custom-call(bf16[3,256]{1,0:T(4,128)(2,1)} %taps.1, bf16[16,128]{1,0:T(8,128)(2,1)} %bitcast.11, bf16[16,128]{1,0:T(8,128)(2,1)} %bitcast.12, bf16[16,128]{1,0:T(8,128)(2,1)} %bitcast.13, s32[4,128]{1,0:T(4,128)} %bitcast.14, f32[4,128]{1,0:T(4,128)} %bitcast.15, bf16[512,256]{1,0:T(8,128)(2,1)} %x_hbm.1, ...), custom_call_target="tpu_custom_call" | custom-call | tf_op jit(solution)/shard_map/pallas_call | solution.py:684
  125.2 0.8 copy.19

commit v3 on v2

--- a/solution.py
+++ b/solution.py
@@ -81,12 +81,12 @@
 
 
 def layer_kernel(
-    taps,
-    mix_gain,
-    pre_gain,
-    post_gain,
-    routes,
-    route_weights,
+    taps_hbm,
+    mix_hbm,
+    pre_hbm,
+    post_hbm,
+    routes_hbm,
+    route_weights_hbm,
     x_hbm,
     gb_hbm,
     gc_hbm,
@@ -99,6 +99,12 @@
     su_hbm,
     sd_hbm,
     out,
+    taps,
+    mix_gain,
+    pre_gain,
+    post_gain,
+    routes,
+    route_weights,
     x_in,
     gb,
     gc,
@@ -198,12 +204,14 @@
         (wu_hbm, wu),
         (wd_hbm, wd),
     )
-    loads = [
-        pltpu.make_async_copy(src, dst, load_sem.at[i]) for i, (src, dst) in enumerate(pairs)
-    ]
-    for load in loads:
-        load.start()
-
+    small = (
+        (routes_hbm, routes),
+        (route_weights_hbm, route_weights),
+        (taps_hbm, taps),
+        (mix_hbm, mix_gain),
+        (pre_hbm, pre_gain),
+        (post_hbm, post_gain),
+    )
     barrier = pltpu.get_barrier_semaphore()
     greeted = [z_peer(by) for by in range(1, Z)]
     greeted += [plane_peer(j)[1] for j in range(1, PLANE)]
@@ -211,8 +219,23 @@
     greeted += [sp_peer(1), sp_peer(-1)]
     for device in greeted:
         pl.semaphore_signal(barrier, inc=1, device_id=device, device_id_type=MESH)
+    loads = [
+        pltpu.make_async_copy(src, dst, load_sem.at[i])
+        for i, (src, dst) in enumerate(pairs + small)
+    ]
+    few = loads[len(pairs) :]
+    loads = loads[: len(pairs)]
+    for load in few:
+        load.start()
+    for load in loads:
+        load.start()
+
+    few[0].wait()
+    few[1].wait()
     fill_tables(meta, routes, route_weights)
     pl.semaphore_wait(barrier, len(greeted))
+    for load in few[2:]:
+        load.wait()
 
     def remote(src, dst, send, recv, device):
         return pltpu.make_async_remote_copy(
@@ -607,7 +630,7 @@
                 group, side = (0, 1) if farthest else (step + 1, way)
                 passed[way, chunk] = begin(gather_copy(src, group, side, chunk, way, step))
             dealt[step] += dispatch(step, chunk, every)
-            if chunk == step - 1 and step > 1:
+            if chunk == 2 * step - 3 and step > 1:
                 finish(dealt[step - 1])
                 experts(step - 1, every)
                 given[step - 1] = give_first(step - 1)
@@ -684,9 +707,15 @@
     return pl.pallas_call(
         layer_kernel,
         out_shape=pltpu.VMEM((tokens, width), bf16),
-        in_specs=[vmem] * 6 + [hbm] * 11,
+        in_specs=[hbm] * 17,
         out_specs=vmem,
         scratch_shapes=[
+            pltpu.VMEM(conv_taps.shape, bf16),
+            pltpu.VMEM((width // 128, 128), bf16),
+            pltpu.VMEM((width // 128, 128), bf16),
+            pltpu.VMEM((width // 128, 128), bf16),
+            pltpu.VMEM(routes.shape[::-1], jnp.int32),
+            pltpu.VMEM(route_weights.shape[::-1], f32),
             pltpu.VMEM((rows, channels), bf16),
             pltpu.VMEM((rows, channels), bf16),
             pltpu.VMEM((rows, channels), bf16),
@@ -714,7 +743,7 @@
             pltpu.VMEM((width, shared), bf16),
             pltpu.VMEM((width, shared), bf16),
             pltpu.VMEM((shared, width), bf16),
-            dma((11,)),
+            dma((17,)),
             dma((2,)),
             dma((2,)),
             dma((2,)),

time: 126 us -> 125 us (level)
  no operation moved by 1% of the time
where the time goes in v3:
time: 125 us
  Pallas kernels  124 us (99%)
    pallas_call x1, Pallas kernels, body(): pl.pallas_call(layer_kernel, out_shape=pltpu.VMEM((tokens, width), bf16),...  124 us

profile of v3, /device:TPU:1, one launch (start us, length us, event | category | flops | bytes accessed | tf_op | source)
XLA Modules:
  0.0 125.2 jit_solution(14423445211546939081)
XLA Ops:
  0.0 124.4 %shard_map.163 = bf16[128,2048]{1,0:T(8,128)(2,1)S(1)} custom-call(bf16[3,256]{1,0:T(4,128)(2,1)} %taps_hbm.1, bf16[16,128]{1,0:T(8,128)(2,1)} %bitcast.11, bf16[16,128]{1,0:T(8,128)(2,1)} %bitcast.12, bf16[16,128]{1,0:T(8,128)(2,1)} %bitcast.13, s32[4,128]{1,0:T(4,128)} %bitcast.14, f32[4,128]{1,0:T(4,128)} %bitcast.15, bf16[512,256]{1,0:T(8,128)(2,1)} %x_hbm.1, ...), custom_call_target="tpu_custom_call" | custom-call | tf_op jit(solution)/shard_map/pallas_call | solution.py:707
  124.4 0.8 copy.19
